TPU v7x, 32 devices: a whole 2x2x4 slice. The times are simulated.
32 devices in a mesh: sp: 8 (over z, y), tp: 4 (over x, core).
Axes of the slice: x: 2, y: 2, z: 4, core: 2. Of those that a mesh axis runs over, the one named last changes fastest.
Arguments:
- tokens: bfloat16 [3072, 2048], P('sp', 'tp'), may hold values from -6 to 6
- norm_gain: float32 [3, 2048], replicated, may hold values from 0.1 to 1.9
- w_value: bfloat16 [3, 2048, 1024], P(None, 'sp', 'tp'), may hold values from -0.125 to 0.125
- w_gate: bfloat16 [3, 2048, 1024], P(None, 'sp', 'tp'), may hold values from -0.125 to 0.125
- conv_taps: float32 [3, 31, 1024], P(None, None, 'tp'), may hold values from -2.4 to 2.4
- conv_bias: float32 [3, 1024], P(None, 'tp'), may hold values from -3 to 3
- ln_gain: float32 [3, 1024], P(None, 'tp'), may hold values from 0.1 to 1.9
- ln_shift: float32 [3, 1024], P(None, 'tp'), may hold values from -3 to 3
- w_out: bfloat16 [3, 1024, 2048], P(None, 'tp', 'sp'), may hold values from -0.1875 to 0.1875
Outputs:
- stream: bfloat16 [3072, 2048], P('sp', 'tp')
All inputs are finite; a program needn't handle non-finite values.
Results may differ from a plain program's by a relative error of at most 0.015.
Values may be sent and summed in bfloat16 or wider, within the bound.
A program may use at most 64 MiB of HBM per device.

v0:
```python
import jax
import jax.numpy as jnp
from jax import lax
from jax.sharding import PartitionSpec as P

norm_floor = 0.01


def with_halo(array, sides, width):
    for axis, dim in sides:
        size, length = (lax.axis_size(axis), array.shape[dim])
        up = [(i, (i + 1) % size) for i in range(size - 1)]
        down = [(j, i) for i, j in up]
        last = lax.slice_in_dim(array, length - width, length, axis=dim)
        first = lax.slice_in_dim(array, 0, width, axis=dim)
        before = lax.ppermute(last, axis, up)
        after = lax.ppermute(first, axis, down)
        array = jnp.concatenate([before, array, after], axis=dim)
    return array


def body(tokens, norm_gain, w_value, w_gate, conv_taps, conv_bias, ln_gain, ln_shift, w_out):
    stream = tokens
    layer_count = w_value.shape[0]
    reach = conv_taps.shape[1] // 2
    local_channels = w_value.shape[2]
    channels = local_channels * lax.axis_size("tp")
    tok_rows = tokens.shape[0]
    whole_value, whole_gate = (
        lax.all_gather(w_value, "sp", axis=1, tiled=True),
        lax.all_gather(w_gate, "sp", axis=1, tiled=True),
    )
    whole_out = lax.all_gather(w_out, "sp", axis=2, tiled=True)
    for layer_index in range(layer_count):
        whole_rows = lax.all_gather(stream, "tp", axis=1, tiled=True)
        rows_f32 = whole_rows.astype(jnp.float32)
        scale_rows = lax.rsqrt(jnp.mean(rows_f32 * rows_f32, axis=-1, keepdims=True) + norm_floor)
        normed = (rows_f32 * scale_rows * norm_gain[layer_index]).astype(jnp.bfloat16)
        value_rows = jnp.dot(normed, whole_value[layer_index], preferred_element_type=jnp.float32)
        gate_rows = jnp.dot(normed, whole_gate[layer_index], preferred_element_type=jnp.float32)
        gated_input = (value_rows * jax.nn.sigmoid(gate_rows)).astype(jnp.bfloat16)
        padded = with_halo(gated_input, (("sp", 0),), reach)
        padded = padded.astype(jnp.float32)
        convolved = jnp.zeros((tok_rows, local_channels), jnp.float32) + conv_bias[layer_index]
        for offset in range(2 * reach + 1):
            convolved = (
                convolved + conv_taps[layer_index, offset] * padded[offset : offset + tok_rows]
            )
        moments = lax.psum(
            (
                jnp.sum(convolved, axis=-1, keepdims=True),
                jnp.sum(convolved * convolved, axis=-1, keepdims=True),
            ),
            "tp",
        )
        average = moments[0] / channels
        spread = moments[1] / channels - average * average
        activated = jax.nn.silu(
            (convolved - average) * lax.rsqrt(spread + norm_floor) * ln_gain[layer_index]
            + ln_shift[layer_index]
        ).astype(jnp.bfloat16)
        partial_rows = jnp.dot(
            activated, whole_out[layer_index], preferred_element_type=jnp.float32
        )
        summed = lax.psum_scatter(
            partial_rows.astype(jnp.bfloat16), "tp", scatter_dimension=1, tiled=True
        ).astype(jnp.float32)
        stream = (stream.astype(jnp.float32) + summed).astype(jnp.bfloat16)
    return stream


def solution(mesh):
    placed = (
        P("sp", "tp"),
        P(),
        P(None, "sp", "tp"),
        P(None, "sp", "tp"),
        P(None, None, "tp"),
        P(None, "tp"),
        P(None, "tp"),
        P(None, "tp"),
        P(None, "tp", "sp"),
    )
    return jax.shard_map(body, mesh=mesh, in_specs=placed, out_specs=P("sp", "tp"), check_vma=False)
```

profile of v0, /device:TPU:0, one launch (start us, length us, event | category | flops | bytes accessed | tf_op | source)
XLA Modules:
  0.0 407.2 jit_solution(14767884248414049821)
XLA Ops:
  6.5 0.7 all-gather.7.cloned.1.call-update
  7.3 0.0 all-gather.11.cloned.1.call-start
  7.3 0.7 all-gather.11.cloned.1.call-update
  8.0 0.0 all-gather.9.cloned.1.call-start
  8.1 0.7 all-gather.9.cloned.1.call-update
  8.7 0.0 all-gather.13.cloned.1.call-start
  8.8 0.5 all-gather.13.cloned.1.call-update
  9.3 0.0 reduce-scatter.4.cloned.1.call-start
  9.4 0.8 fusion.155
  10.2 0.8 fusion.153
  11.0 1.0 fusion.151
  12.0 1.1 fusion.150
  13.0 0.9 fusion.152
  13.9 17.3 %all-gather.7.cloned.1.call-done = bf16[384,2048]{1,0:T(8,128)(2,1)} async-done(((bf16[384,512]{1,0:T(8,128)(2,1)}), bf16[384,2048]{1,0:T(8,128)(2,1)}) %all-gather.7.cloned.1.call-update) | async-done | bytes 1572880 | tf_op jit(solution)/shard_map/all_gather | solution.py:35
  31.3 1.8 fusion
  33.1 60.4 %all-gather.11.cloned.1.call-done = bf16[3,2048,256]{2,1,0:T(8,128)(2,1)} async-done(((bf16[3,256,256]{2,1,0:T(8,128)(2,1)}), bf16[3,2048,256]{2,1,0:T(8,128)(2,1)}) %all-gather.11.cloned.1.call-update) | async-done | bytes 3145744 | tf_op jit(solution)/shard_map/all_gather | solution.py:31
  93.5 2.5 fusion.13
  96.0 0.0 copy-start.7
  96.0 58.4 %all-gather.9.cloned.1.call-done = bf16[3,2048,256]{2,1,0:T(8,128)(2,1)} async-done(((bf16[3,256,256]{2,1,0:T(8,128)(2,1)}), bf16[3,2048,256]{2,1,0:T(8,128)(2,1)}) %all-gather.9.cloned.1.call-update) | async-done | bytes 3145744 | tf_op jit(solution)/shard_map/all_gather | solution.py:30
  154.4 1.9 fusion.18
  156.3 2.5 collective-permute-start
  158.8 1.3 collective-permute-start.1
  160.1 0.0 collective-permute-done
  160.1 4.6 %collective-permute-done.1 = bf16[15,256]{1,0:T(8,128)(2,1)S(1)} collective-permute-done((bf16[15,256]{1,0:T(8,128)(2,1)S(1)}, bf16[15,256]{1,0:T(8,128)(2,1)S(1)}, u32[]{:S(2)}, u32[]{:S(2)}) %collective-permute-start.1) | collective-permute-done | bytes 7712 | tf_op jit(solution)/shard_map/ppermute | solution.py:17
  164.7 1.7 fusion.140
  166.4 6.2 %all-reduce.2 = (f32[384,1]{0,1:T(1,128)S(1)}, f32[384,1]{0,1:T(1,128)S(1)}) all-reduce(f32[384,1]{0,1:T(1,128)S(1)} %broadcast_in_dim.21, f32[384,1]{0,1:T(1,128)S(1)} %broadcast_in_dim.22), channel_id=1, replica_groups=mesh['sp'=8,'tp'=4] {'tp'}, use_global_device_ids=true, to_apply=%region_2.0 | all-reduce | flops 768 | bytes 6144 | tf_op jit(solution)/shard_map/psum | solution.py:49
  172.7 45.0 %all-gather.13.cloned.1.call-done = bf16[3,256,2048]{2,1,0:T(8,128)(2,1)} async-done(((bf16[3,256,256]{2,1,0:T(8,128)(2,1)}), bf16[3,256,2048]{2,1,0:T(8,128)(2,1)}) %all-gather.13.cloned.1.call-update) | async-done | bytes 3145744 | tf_op jit(solution)/shard_map/all_gather | solution.py:33
  217.7 3.1 convolution_convert_fusion.2
  220.8 0.0 reduce-scatter.4.cloned.1.call-update
  220.8 0.0 all-gather.15.cloned.1.call-start
  220.8 26.3 %reduce-scatter.4.cloned.1.call-done = bf16[384,512]{1,0:T(8,128)(2,1)} async-done(((bf16[384,2048]{1,0:T(8,128)(2,1)}), bf16[384,512]{1,0:T(8,128)(2,1)}) %reduce-scatter.4.cloned.1.call-update) | async-done | bytes 393232 | tf_op jit(solution)/shard_map/reduce_scatter | solution.py:65
  247.2 1.8 add_convert_fusion.2
  249.0 0.0 all-gather.15.cloned.1.call-update
  249.0 0.0 reduce-scatter.6.cloned.1.call-start
  249.1 19.7 %all-gather.15.cloned.1.call-done = bf16[384,2048]{1,0:T(8,128)(2,1)} async-done(((bf16[384,512]{1,0:T(8,128)(2,1)}), bf16[384,2048]{1,0:T(8,128)(2,1)}) %all-gather.15.cloned.1.call-update) | async-done | bytes 1572880 | tf_op jit(solution)/shard_map/all_gather | solution.py:35
  268.8 1.8 fusion.3
  270.6 2.5 fusion.15
  273.1 1.9 fusion.19
  275.0 3.4 collective-permute-start.2
  278.4 1.3 collective-permute-start.3
  279.7 0.0 collective-permute-done.2
  279.7 4.2 %collective-permute-done.3 = bf16[15,256]{1,0:T(8,128)(2,1)S(1)} collective-permute-done((bf16[15,256]{1,0:T(8,128)(2,1)S(1)}, bf16[15,256]{1,0:T(8,128)(2,1)S(1)}, u32[]{:S(2)}, u32[]{:S(2)}) %collective-permute-start.3) | collective-permute-done | bytes 7712 | tf_op jit(solution)/shard_map/ppermute | solution.py:17
  284.0 1.7 fusion.139
  285.7 6.1 %all-reduce.1 = (f32[384,1]{0,1:T(1,128)S(1)}, f32[384,1]{0,1:T(1,128)S(1)}) all-reduce(f32[384,1]{0,1:T(1,128)S(1)} %broadcast_in_dim.23, f32[384,1]{0,1:T(1,128)S(1)} %broadcast_in_dim.24), channel_id=1, replica_groups=mesh['sp'=8,'tp'=4] {'tp'}, use_global_device_ids=true, to_apply=%region_8.9 | all-reduce | flops 768 | bytes 6144 | tf_op jit(solution)/shard_map/psum | solution.py:49
  291.8 3.1 convolution_convert_fusion.1
  294.8 0.0 reduce-scatter.6.cloned.1.call-update
  294.9 0.0 all-gather.17.cloned.1.call-start
  294.9 28.1 %reduce-scatter.6.cloned.1.call-done = bf16[384,512]{1,0:T(8,128)(2,1)} async-done(((bf16[384,2048]{1,0:T(8,128)(2,1)}), bf16[384,512]{1,0:T(8,128)(2,1)}) %reduce-scatter.6.cloned.1.call-update) | async-done | bytes 393232 | tf_op jit(solution)/shard_map/reduce_scatter | solution.py:65
  323.0 1.8 add_convert_fusion.1
  324.8 0.0 all-gather.17.cloned.1.call-update
  324.9 0.0 reduce-scatter.8.cloned.1.call-start
  324.9 19.7 %all-gather.17.cloned.1.call-done = bf16[384,2048]{1,0:T(8,128)(2,1)} async-done(((bf16[384,512]{1,0:T(8,128)(2,1)}), bf16[384,2048]{1,0:T(8,128)(2,1)}) %all-gather.17.cloned.1.call-update) | async-done | bytes 1572880 | tf_op jit(solution)/shard_map/all_gather | solution.py:35
  344.6 1.8 fusion.6
  346.4 2.5 fusion.17
  348.9 1.9 fusion.20
  350.8 3.4 collective-permute-start.4
  354.2 1.5 collective-permute-start.5
  355.7 4.0 collective-permute-done.5
  359.8 1.7 fusion.138
  361.5 6.1 %all-reduce = (f32[384,1]{0,1:T(1,128)S(1)}, f32[384,1]{0,1:T(1,128)S(1)}) all-reduce(f32[384,1]{0,1:T(1,128)S(1)} %broadcast_in_dim.25, f32[384,1]{0,1:T(1,128)S(1)} %broadcast_in_dim.26), channel_id=1, replica_groups=mesh['sp'=8,'tp'=4] {'tp'}, use_global_device_ids=true, to_apply=%region_14.15 | all-reduce | flops 768 | bytes 6144 | tf_op jit(solution)/shard_map/psum | solution.py:49
  367.6 3.0 convolution_convert_fusion
  370.6 0.0 reduce-scatter.8.cloned.1.call-update
  370.7 28.2 %reduce-scatter.8.cloned.1.call-done = bf16[384,512]{1,0:T(8,128)(2,1)} async-done(((bf16[384,2048]{1,0:T(8,128)(2,1)}), bf16[384,512]{1,0:T(8,128)(2,1)}) %reduce-scatter.8.cloned.1.call-update) | async-done | bytes 393232 | tf_op jit(solution)/shard_map/reduce_scatter | solution.py:65
  398.9 1.8 add_convert_fusion
  (39 shorter events, 0.4 us)
Async XLA Ops:
  6.5 24.7 %all-gather.7.cloned.1.call-start = ((), (), s32[]{:S(2)}) async-start(), calls=%async_computation.3 | async-start | bytes 1966080 | tf_op jit(solution)/shard_map/all_gather | solution.py:35
  7.3 86.3 %all-gather.11.cloned.1.call-start = ((), (), s32[]{:S(2)}) async-start(), calls=%async_computation.5 | async-start | bytes 3538944 | tf_op jit(solution)/shard_map/all_gather | solution.py:31
  8.0 146.4 %all-gather.9.cloned.1.call-start = ((), (), s32[]{:S(2)}) async-start(), calls=%async_computation.4 | async-start | bytes 3538944 | tf_op jit(solution)/shard_map/all_gather | solution.py:30
  8.7 208.9 %all-gather.13.cloned.1.call-start = ((), (), s32[]{:S(2)}) async-start(), calls=%async_computation.6 | async-start | bytes 3538944 | tf_op jit(solution)/shard_map/all_gather | solution.py:33
  9.3 237.9 %reduce-scatter.4.cloned.1.call-start = ((), (), s32[]{:S(2)}) async-start(), calls=%async_computation.7 | async-start | bytes 1966080 | tf_op jit(solution)/shard_map/reduce_scatter | solution.py:65
  93.5 60.9 %copy-start.2 = (bf16[384,2048]{1,0:T(8,128)(2,1)S(1)}, bf16[384,2048]{1,0:T(8,128)(2,1)}, u32[]{:S(2)}) copy-start(bf16[384,2048]{1,0:T(8,128)(2,1)} %all-gather.7.cloned.1.call-done) | copy-start | bytes 4718596
  96.0 64.1 %copy-start.7 = (f32[3,256]{1,0:T(4,128)S(1)}, f32[3,256]{1,0:T(4,128)}, u32[]{:S(2)}) copy-start(f32[3,256]{1,0:T(4,128)} %param.16) | copy-start | bytes 9220
  156.3 3.8 collective-permute-start
  158.8 5.9 %collective-permute-start.1 = (bf16[15,256]{1,0:T(8,128)(2,1)S(1)}, bf16[15,256]{1,0:T(8,128)(2,1)S(1)}, u32[]{:S(2)}, u32[]{:S(2)}) collective-permute-start(bf16[15,256]{1,0:T(8,128)(2,1)S(1)} %get-tuple-element.31), channel_id=1, source_target_pairs={{4,0},{8,4},{12,8},{16,12},{20,16},{24,20},{28,24},{5,1},{9,5},{13... | collective-permute-start | bytes 23048 | tf_op jit(solution)/shard_map/ppermute | solution.py:17
  166.4 80.7 %copy-start.5 = (bf16[384,512]{1,0:T(8,128)(2,1)S(1)}, bf16[384,512]{1,0:T(8,128)(2,1)}, u32[]{:S(2)}) copy-start(bf16[384,512]{1,0:T(8,128)(2,1)} %param.9) | copy-start | bytes 1179652
  217.7 31.4 %copy-start.6 = (f32[3,31,256]{2,1,0:T(8,128)S(1)}, f32[3,31,256]{2,1,0:T(8,128)}, u32[]{:S(2)}) copy-start(f32[3,31,256]{2,1,0:T(8,128)} %param.13) | copy-start | bytes 285700
  220.8 48.0 %all-gather.15.cloned.1.call-start = ((), (), s32[]{:S(2)}) async-start(), calls=%async_computation.8 | async-start | bytes 1966080 | tf_op jit(solution)/shard_map/all_gather | solution.py:35
  249.0 74.0 %reduce-scatter.6.cloned.1.call-start = ((), (), s32[]{:S(2)}) async-start(), calls=%async_computation.9 | async-start | bytes 1966080 | tf_op jit(solution)/shard_map/reduce_scatter | solution.py:65
  270.6 2.5 copy-start.3
  275.0 4.7 %collective-permute-start.2 = (bf16[15,256]{1,0:T(8,128)(2,1)S(1)}, bf16[15,256]{1,0:T(8,128)(2,1)S(1)}, u32[]{:S(2)}, u32[]{:S(2)}) collective-permute-start(bf16[15,256]{1,0:T(8,128)(2,1)S(1)} %get-tuple-element.28), channel_id=1, source_target_pairs={{0,4},{4,8},{8,12},{12,16},{16,20},{20,24},{24,28},{1,5},{5,9},{9,... | collective-permute-start | bytes 23048 | tf_op jit(solution)/shard_map/ppermute | solution.py:16
  278.4 5.5 %collective-permute-start.3 = (bf16[15,256]{1,0:T(8,128)(2,1)S(1)}, bf16[15,256]{1,0:T(8,128)(2,1)S(1)}, u32[]{:S(2)}, u32[]{:S(2)}) collective-permute-start(bf16[15,256]{1,0:T(8,128)(2,1)S(1)} %get-tuple-element.29), channel_id=1, source_target_pairs={{4,0},{8,4},{12,8},{16,12},{20,16},{24,20},{28,24},{5,1},{9,5},{13... | collective-permute-start | bytes 23048 | tf_op jit(solution)/shard_map/ppermute | solution.py:17
  285.7 37.3 %copy-start = (bf16[384,512]{1,0:T(8,128)(2,1)S(1)}, bf16[384,512]{1,0:T(8,128)(2,1)}, u32[]{:S(2)}) copy-start(bf16[384,512]{1,0:T(8,128)(2,1)} %add_convert_fusion.2) | copy-start | bytes 1179652
  294.9 49.8 %all-gather.17.cloned.1.call-start = ((), (), s32[]{:S(2)}) async-start(), calls=%async_computation.10 | async-start | bytes 1966080 | tf_op jit(solution)/shard_map/all_gather | solution.py:35
  324.9 74.0 %reduce-scatter.8.cloned.1.call-start = ((), (), s32[]{:S(2)}) async-start(), calls=%async_computation.11 | async-start | bytes 1966080 | tf_op jit(solution)/shard_map/reduce_scatter | solution.py:65
  346.4 2.5 copy-start.4
  350.8 4.9 %collective-permute-start.4 = (bf16[15,256]{1,0:T(8,128)(2,1)S(1)}, bf16[15,256]{1,0:T(8,128)(2,1)S(1)}, u32[]{:S(2)}, u32[]{:S(2)}) collective-permute-start(bf16[15,256]{1,0:T(8,128)(2,1)S(1)} %get-tuple-element.26), channel_id=1, source_target_pairs={{0,4},{4,8},{8,12},{12,16},{16,20},{20,24},{24,28},{1,5},{5,9},{9,... | collective-permute-start | bytes 23048 | tf_op jit(solution)/shard_map/ppermute | solution.py:16
  354.2 5.5 %collective-permute-start.5 = (bf16[15,256]{1,0:T(8,128)(2,1)S(1)}, bf16[15,256]{1,0:T(8,128)(2,1)S(1)}, u32[]{:S(2)}, u32[]{:S(2)}) collective-permute-start(bf16[15,256]{1,0:T(8,128)(2,1)S(1)} %get-tuple-element.27), channel_id=1, source_target_pairs={{4,0},{8,4},{12,8},{16,12},{20,16},{24,20},{28,24},{5,1},{9,5},{13... | collective-permute-start | bytes 23048 | tf_op jit(solution)/shard_map/ppermute | solution.py:17
  361.5 37.4 %copy-start.1 = (bf16[384,512]{1,0:T(8,128)(2,1)S(1)}, bf16[384,512]{1,0:T(8,128)(2,1)}, u32[]{:S(2)}) copy-start(bf16[384,512]{1,0:T(8,128)(2,1)} %add_convert_fusion.1) | copy-start | bytes 1179652
Sparse Core Ops, SparseCore 0:
  8.9 22.3 all-gather.6
  33.5 60.0 all-gather.10
  95.7 58.6 all-gather.8
  156.3 61.2 all-gather.12
  220.9 26.2 reduce-scatter.3
  249.2 19.6 all-gather.14
  295.0 27.9 reduce-scatter.5
  325.0 19.6 all-gather.16
  370.8 28.0 reduce-scatter.7
where the time goes:
time: 408 us; the launch traced here: 407 us
  waiting for transfers between devices  319 us (78%)
  matrix products  22.1 us (5%)
  blocking collectives  18.4 us (5%)
  other arithmetic  16.2 us (4%)
  starting transfers between devices  13.6 us (3%)
  between operations  13.5 us (3%)
  local copies, waits for them, and re-layouts  4.71 us (1%)
    reduce_scatter x3, waiting for transfers between devices, body(): lax.psum_scatter(partial_rows.astype(jnp.bfloat16), 'tp', scatter_dimensi...  82.6 us
    all_gather x1, waiting for transfers between devices, body(): lax.all_gather(w_gate, 'sp', axis=1, tiled=True)  60.4 us
    all_gather x1, waiting for transfers between devices, body(): lax.all_gather(w_value, 'sp', axis=1, tiled=True)  58.4 us
    all_gather x3, waiting for transfers between devices, body(): whole_rows = lax.all_gather(stream, 'tp', axis=1, tiled=True)  56.8 us
    all_gather x1, waiting for transfers between devices, body(): whole_out = lax.all_gather(w_out, 'sp', axis=2, tiled=True)  45 us
    psum x3, blocking collectives, body(): lax.psum((jnp.sum(convolved, axis=-1, keepdims=True), jnp.sum(convolved *...  18.4 us
    ppermute x3, waiting for transfers between devices, with_halo(): after = lax.ppermute(first, axis, down)  12.8 us
    ppermute x3, starting transfers between devices, with_halo(): before = lax.ppermute(last, axis, up)  9.21 us
  transfers between devices with their start and end apart: 15, of which 12 were waited for; matrix products, arithmetic and copies ran while one was open for 3% of the time, Pallas kernels for 0%

commit v1 on v0

--- a/solution.py
+++ b/solution.py
@@ -1,7 +1,13 @@
+import functools
+
 import jax
 import jax.numpy as jnp
 from jax import lax
+from jax.experimental import pallas as pl
+from jax.experimental.pallas import tpu as pltpu
 from jax.sharding import PartitionSpec as P
+
+MESH = pl.DeviceIdType.MESH
 
 norm_floor = 0.01
 
@@ -69,6 +75,432 @@
     return stream
 
 
+def fused(
+    dims,
+    tok, gain_in, wv_in, wg_in, wo_in, taps_in, bias_in, lng_in, lns_in,
+    out,
+    wvg, wo, taps, bias, lng, lns, stream, gated, conv, acc1, acc2, act,
+    part_out, part_in, stat_out, stat_in, stat_m, final_out, final_in,
+    loc_sem, ring_send, ring_recv, pair_send, pair_recv,
+    tok_send, tok_recv, halo_send, halo_recv, par_send, par_recv,
+    px_send, px_recv, st_send, st_recv, fin_send, fin_recv,
+):
+    n, tp, layers, ntaps, rows, width, chans, pieces = dims
+    feats = width // tp
+    drows = width // n
+    ocols = width // n
+    lch = chans // tp
+    pch = 2 * lch
+    half_rows = rows // 2
+    reach = ntaps // 2
+    grain = 16
+    halo = grain * layers
+    window = half_rows + 2 * halo
+    main = half_rows + halo
+    m = n // 2
+    half_feats = width // 2
+
+    sp = lax.axis_index("sp")
+    t = lax.axis_index("tp")
+    h = lax.rem(t, 2)
+    xg = t // 2
+    pair = t + 1 - 2 * h
+    across = lax.rem(t + 2, tp)
+    odd = lax.rem(sp, 2)
+    pos = (1 - odd) * (sp // 2) + odd * (n - (sp + 1) // 2)
+
+    def ring_sp(p):
+        p = lax.rem(p + 2 * n, n)
+        q = p // m
+        return (1 - q) * (2 * p) + q * (2 * (n - p) - 1)
+
+    right, left = ring_sp(pos + 1), ring_sp(pos - 1)
+    up, down = lax.rem(sp + 1, n), lax.rem(sp + n - 1, n)
+
+    barrier = pltpu.get_barrier_semaphore()
+    greet = [(sp, lax.rem(t + j, tp)) for j in range(1, tp)]
+    greet += [(up, j) for j in range(tp)] + [(down, j) for j in range(tp)]
+    greet += [(right, t), (left, t)]
+
+    def block(layer, kind, origin, side, half=None):
+        if kind == 0:
+            r = pl.ds(pl.multiple_of(origin * drows, drows), drows)
+            if half is None:
+                return wvg.at[layer, side, :, r, :]
+            return wvg.at[layer, side, half, r, :]
+        c = pl.ds(pl.multiple_of(origin * ocols, ocols), ocols)
+        if half is None:
+            return wo.at[layer, pl.ds(pl.multiple_of(side * lch, lch), lch), c]
+        hl = lch // 2
+        return wo.at[layer, pl.ds(pl.multiple_of(side * lch + half * hl, hl), hl), c]
+
+    def local_copies(layer, kind):
+        if kind == 0:
+            r = pl.ds(pl.multiple_of(sp * drows, drows), drows)
+            return [
+                pltpu.make_async_copy(wv_in.at[layer], wvg.at[layer, h, 0, r, :], loc_sem.at[3 * layer]),
+                pltpu.make_async_copy(wg_in.at[layer], wvg.at[layer, h, 1, r, :], loc_sem.at[3 * layer + 1]),
+            ]
+        return [pltpu.make_async_copy(wo_in.at[layer], block(layer, 1, sp, h), loc_sem.at[3 * layer + 2])]
+
+    def ring_copy(layer, kind, direction, step):
+        shift = -(step - 1) if direction == 0 else step - 1
+        half = direction if step == m else None
+        ref = block(layer, kind, ring_sp(pos + shift), h, half)
+        i = ((layer * 2 + kind) * 2 + direction) * m + step - 1
+        return pltpu.make_async_remote_copy(
+            src_ref=ref, dst_ref=ref, send_sem=ring_send.at[i], recv_sem=ring_recv.at[i],
+            device_id=(right if direction == 0 else left, t), device_id_type=MESH)
+
+    def ring_arrival(layer, kind, direction, step, side):
+        shift = -step if direction == 0 else step
+        half = direction if step == m else None
+        return block(layer, kind, ring_sp(pos + shift), side, half)
+
+    def pair_copy(layer, kind, direction, step, side):
+        if step == 0:
+            ref, j = block(layer, kind, sp, side), 0
+        else:
+            ref, j = ring_arrival(layer, kind, direction, step, side), direction * m + step
+        i = (layer * 2 + kind) * (2 * m + 1) + j
+        return pltpu.make_async_remote_copy(
+            src_ref=ref, dst_ref=ref, send_sem=pair_send.at[i], recv_sem=pair_recv.at[i],
+            device_id=(sp, pair), device_id_type=MESH)
+
+    def send_own(layer, kind):
+        for c in local_copies(layer, kind):
+            c.wait()
+        for d in range(2):
+            ring_copy(layer, kind, d, 1).start()
+        pair_copy(layer, kind, 0, 0, h).start()
+
+    def relay(layer, kind, step):
+        for d in range(2):
+            ref = ring_arrival(layer, kind, d, step, h)
+            i = ((layer * 2 + kind) * 2 + d) * m + step - 1
+            pltpu.make_async_remote_copy(
+                src_ref=ref, dst_ref=ref, send_sem=ring_send.at[i], recv_sem=ring_recv.at[i],
+                device_id=(right, t), device_id_type=MESH).wait_recv()
+            if step < m:
+                ring_copy(layer, kind, d, step + 1).start()
+            pair_copy(layer, kind, d, step, h).start()
+
+    def pair_wait(layer, kind):
+        pair_copy(layer, kind, 0, 0, 1 - h).wait_recv()
+        for step in range(1, m + 1):
+            for d in range(2):
+                pair_copy(layer, kind, d, step, 1 - h).wait_recv()
+
+    tcols = pl.ds(pl.multiple_of(t * feats, feats), feats)
+
+    def window_cols(owner):
+        return pl.ds(pl.multiple_of(owner * feats, feats), feats)
+
+    def tok_copy(j):
+        dest = lax.rem(t + j, tp)
+        dh = lax.rem(dest, 2)
+        return pltpu.make_async_remote_copy(
+            src_ref=tok.at[pl.ds(pl.multiple_of(dh * (rows - main), grain), main), :],
+            dst_ref=stream.at[pl.ds(pl.multiple_of((1 - dh) * halo, grain), main), tcols],
+            send_sem=tok_send.at[j - 1], recv_sem=tok_recv.at[j - 1],
+            device_id=(sp, dest), device_id_type=MESH)
+
+    def tok_wait(j):
+        owner = lax.rem(t + tp - j, tp)
+        ref = stream.at[pl.ds(pl.multiple_of((1 - h) * halo, grain), main), window_cols(owner)]
+        return pltpu.make_async_remote_copy(
+            src_ref=ref, dst_ref=ref, send_sem=tok_send.at[j - 1], recv_sem=tok_recv.at[j - 1],
+            device_id=(sp, pair), device_id_type=MESH)
+
+    def halo_copies():
+        for g in range(tp // 2):
+            yield pltpu.make_async_remote_copy(
+                src_ref=tok.at[pl.ds(rows - halo, halo), :], dst_ref=stream.at[pl.ds(0, halo), tcols],
+                send_sem=halo_send.at[2 * g], recv_sem=halo_recv.at[t],
+                device_id=(up, 2 * g), device_id_type=MESH)
+            yield pltpu.make_async_remote_copy(
+                src_ref=tok.at[pl.ds(0, halo), :], dst_ref=stream.at[pl.ds(main, halo), tcols],
+                send_sem=halo_send.at[2 * g + 1], recv_sem=halo_recv.at[t],
+                device_id=(down, 2 * g + 1), device_id_type=MESH)
+
+    def halo_wait(owner):
+        ref = stream.at[pl.ds(pl.multiple_of(h * main, grain), halo), owner * feats:(owner + 1) * feats]
+        return pltpu.make_async_remote_copy(
+            src_ref=ref, dst_ref=ref, send_sem=halo_send.at[0], recv_sem=halo_recv.at[owner],
+            device_id=(sp, pair), device_id_type=MESH)
+
+    def param_copies():
+        for i, (a, b) in enumerate(((taps_in, taps), (bias_in, bias), (lng_in, lng), (lns_in, lns))):
+            yield pltpu.make_async_remote_copy(
+                src_ref=a, dst_ref=b.at[h], send_sem=par_send.at[i], recv_sem=par_recv.at[i],
+                device_id=(sp, pair), device_id_type=MESH)
+
+    def param_waits():
+        for i, (a, b) in enumerate(((taps_in, taps), (bias_in, bias), (lng_in, lng), (lns_in, lns))):
+            yield pltpu.make_async_remote_copy(
+                src_ref=a, dst_ref=b.at[1 - h], send_sem=par_send.at[i], recv_sem=par_recv.at[i],
+                device_id=(sp, pair), device_id_type=MESH)
+
+    for layer in range(layers):
+        for kind in range(2):
+            for c in local_copies(layer, kind):
+                c.start()
+    for dev in greet:
+        pl.semaphore_signal(barrier, inc=1, device_id=dev, device_id_type=MESH)
+    pl.semaphore_wait(barrier, len(greet))
+
+    for c in halo_copies():
+        c.start()
+    for j in range(1, tp):
+        tok_copy(j).start()
+    send_own(0, 0)
+    for c in param_copies():
+        c.start()
+    send_own(0, 1)
+
+    stream[pl.ds(pl.multiple_of((1 - h) * halo, grain), main), tcols] = tok[
+        pl.ds(pl.multiple_of(h * (rows - main), grain), main), :]
+    taps[h] = taps_in[...]
+    bias[h] = bias_in[...]
+    lng[h] = lng_in[...]
+    lns[h] = lns_in[...]
+    stat_m[...] = jnp.zeros_like(stat_m)
+
+    first_row = sp * rows + h * half_rows - halo
+    total_rows = n * rows
+
+    def project(layer, start, size):
+        x = stream[pl.ds(start, size), :].astype(jnp.float32)
+        scale = lax.rsqrt(jnp.mean(x * x, axis=-1, keepdims=True) + norm_floor)
+        normed = (x * scale * gain_in[layer:layer + 1, :]).astype(jnp.bfloat16)
+        row = lax.broadcasted_iota(jnp.int32, (size, lch), 0) + (first_row + start)
+        inside = jnp.logical_and(row >= 0, row < total_rows)
+        for c in range(2):
+            value = jnp.dot(normed, wvg[layer, c, 0], preferred_element_type=jnp.float32)
+            gate = jnp.dot(normed, wvg[layer, c, 1], preferred_element_type=jnp.float32)
+            g = (value * jax.nn.sigmoid(gate)).astype(jnp.bfloat16).astype(jnp.float32)
+            gated[pl.ds(start, size), c * lch:(c + 1) * lch] = jnp.where(inside, g, 0.0)
+
+    def convolve(layer, start, size):
+        lanes_per = 128
+        per_side = lch // lanes_per
+        acc1[...] = jnp.zeros_like(acc1)
+        acc2[...] = jnp.zeros_like(acc2)
+
+        def lane_block(b, carry):
+            c = b // per_side
+            lane = pl.ds(pl.multiple_of(lax.rem(b, per_side) * lanes_per, lanes_per), lanes_per)
+            wide = pl.ds(pl.multiple_of(b * lanes_per, lanes_per), lanes_per)
+            for r0 in range(0, size, 112 if size % 112 == 0 else (96 if size % 96 == 0 else 128)):
+                rs = 112 if size % 112 == 0 else (96 if size % 96 == 0 else 128)
+                total = jnp.zeros((rs, lanes_per), jnp.float32) + bias[c, layer:layer + 1, lane]
+                for k in range(ntaps):
+                    total = total + taps[c, layer, k:k + 1, lane] * gated[
+                        start + r0 + k - reach:start + r0 + k - reach + rs, wide]
+                conv[r0:r0 + rs, wide] = total
+                acc1[r0:r0 + rs, :] += total
+                acc2[r0:r0 + rs, :] += total * total
+            return carry
+
+        lax.fori_loop(0, 2 * per_side, lane_block, 0)
+
+    def stat_copy(layer):
+        return pltpu.make_async_remote_copy(
+            src_ref=stat_out.at[layer], dst_ref=stat_in.at[layer], send_sem=st_send.at[layer],
+            recv_sem=st_recv.at[layer], device_id=(sp, across), device_id_type=MESH)
+
+    def part_copy(layer, i, r0, size, last):
+        r = pl.ds(r0, size)
+        if last:
+            src = part_out.at[layer, r, pl.ds(pl.multiple_of((1 - xg) * half_feats, half_feats), half_feats)]
+            dst = part_in.at[layer, r, pl.ds(pl.multiple_of((1 - xg) * half_feats, half_feats), half_feats)]
+        else:
+            src, dst = part_out.at[layer, r, :], part_in.at[layer, r, :]
+        return pltpu.make_async_remote_copy(
+            src_ref=src, dst_ref=dst, send_sem=px_send.at[layer * pieces + i],
+            recv_sem=px_recv.at[layer * pieces + i], device_id=(sp, across), device_id_type=MESH)
+
+    for step in range(1, m + 1):
+        relay(0, 0, step)
+    for j in range(1, tp):
+        tok_wait(j).wait_recv()
+    for owner in range(tp):
+        halo_wait(owner).wait_recv()
+    pair_wait(0, 0)
+    if layers > 1:
+        send_own(1, 0)
+    for i in range(2):
+        project(0, i * (window // 2), window // 2)
+    for c in param_waits():
+        c.wait_recv()
+
+    for layer in range(layers):
+        last = layer == layers - 1
+        start = grain * (layer + 1)
+        size = window - 2 * start
+        convolve(layer, start, size)
+        lane_id = lax.broadcasted_iota(jnp.int32, (size, 128), 1)
+        s1 = jnp.sum(acc1[0:size, :], axis=-1, keepdims=True)
+        s2 = jnp.sum(acc2[0:size, :], axis=-1, keepdims=True)
+        stat_m[0:size, :] = jnp.where(lane_id == 0, s1, jnp.where(lane_id == 1, s2, 0.0))
+        mine = jnp.transpose(stat_m[...])
+        stat_out[layer] = mine[0:8, :]
+        stat_copy(layer).start()
+        for step in range(1, m + 1):
+            relay(layer, 1, step)
+        if layer + 1 < layers:
+            send_own(layer + 1, 1)
+        stat_copy(layer).wait_recv()
+        both = stat_out[layer] + stat_in[layer]
+        wide = jnp.concatenate([both, jnp.zeros((120, both.shape[1]), jnp.float32)], axis=0)
+        stat_m[...] = jnp.transpose(wide)
+        pair_wait(layer, 1)
+        piece = size // pieces
+        for i in range(pieces):
+            r0 = i * piece
+            average = stat_m[r0:r0 + piece, 0:1] / chans
+            spread = stat_m[r0:r0 + piece, 1:2] / chans - average * average
+            scale = lax.rsqrt(spread + norm_floor)
+            for c in range(2):
+                y = (conv[r0:r0 + piece, c * lch:(c + 1) * lch] - average) * scale
+                y = y * lng[c, layer:layer + 1, :] + lns[c, layer:layer + 1, :]
+                act[r0:r0 + piece, c * lch:(c + 1) * lch] = (y / (1.0 + jnp.exp(-y))).astype(jnp.bfloat16)
+            part_out[layer, r0:r0 + piece, :] = jnp.dot(
+                act[r0:r0 + piece, :], wo[layer], preferred_element_type=jnp.float32).astype(jnp.bfloat16)
+            part_copy(layer, i, r0, piece, last).start()
+        if not last:
+            for step in range(1, m + 1):
+                relay(layer + 1, 0, step)
+            pair_wait(layer + 1, 0)
+            if layer + 2 < layers:
+                send_own(layer + 2, 0)
+            for i in range(pieces):
+                r0 = i * piece
+                part_copy(layer, i, r0, piece, last).wait_recv()
+                w0 = start + r0
+                stream[w0:w0 + piece, :] = (
+                    stream[w0:w0 + piece, :].astype(jnp.float32)
+                    + part_out[layer, r0:r0 + piece, :].astype(jnp.float32)
+                    + part_in[layer, r0:r0 + piece, :].astype(jnp.float32)).astype(jnp.bfloat16)
+                project(layer + 1, w0, piece)
+        else:
+            mycols = pl.ds(pl.multiple_of(xg * half_feats, half_feats), half_feats)
+
+            def fin_copy(i, r0):
+                return pltpu.make_async_remote_copy(
+                    src_ref=final_out.at[pl.ds(r0, piece), pl.ds(pl.multiple_of((1 - h) * feats, feats), feats)],
+                    dst_ref=final_in.at[pl.ds(r0, piece), :],
+                    send_sem=fin_send.at[i], recv_sem=fin_recv.at[i],
+                    device_id=(sp, pair), device_id_type=MESH)
+
+            for i in range(pieces):
+                r0 = i * piece
+                ref = part_in.at[layer, pl.ds(r0, piece), mycols]
+                pltpu.make_async_remote_copy(
+                    src_ref=ref, dst_ref=ref, send_sem=px_send.at[layer * pieces + i],
+                    recv_sem=px_recv.at[layer * pieces + i], device_id=(sp, across),
+                    device_id_type=MESH).wait_recv()
+                w0 = start + r0
+                final_out[r0:r0 + piece, :] = (
+                    stream[w0:w0 + piece, mycols].astype(jnp.float32)
+                    + part_out[layer, r0:r0 + piece, mycols].astype(jnp.float32)
+                    + part_in[layer, r0:r0 + piece, mycols].astype(jnp.float32)).astype(jnp.bfloat16)
+                fin_copy(i, r0).start()
+            out[pl.ds(pl.multiple_of(h * half_rows, grain), half_rows), :] = final_out[
+                :, pl.ds(pl.multiple_of(h * feats, feats), feats)]
+            for i in range(pieces):
+                fin_copy(i, i * piece).wait_recv()
+            out[pl.ds(pl.multiple_of((1 - h) * half_rows, grain), half_rows), :] = final_in[...]
+            for i in range(pieces):
+                fin_copy(i, i * piece).wait_send()
+
+    for c in halo_copies():
+        c.wait_send()
+    for j in range(1, tp):
+        tok_copy(j).wait_send()
+    for c in param_copies():
+        c.wait_send()
+    for layer in range(layers):
+        last = layer == layers - 1
+        size = window - 2 * grain * (layer + 1)
+        piece = size // pieces
+        stat_copy(layer).wait_send()
+        for i in range(pieces):
+            part_copy(layer, i, i * piece, piece, last).wait_send()
+        for kind in range(2):
+            pair_copy(layer, kind, 0, 0, h).wait_send()
+            for step in range(1, m + 1):
+                for d in range(2):
+                    ring_copy(layer, kind, d, step).wait_send()
+                    pair_copy(layer, kind, d, step, h).wait_send()
+
+
+def fused_call(mesh, *args):
+    tokens, norm_gain, w_value, w_gate, conv_taps, conv_bias, ln_gain, ln_shift, w_out = args
+    n, tp = mesh.shape["sp"], mesh.shape["tp"]
+    layers, ntaps, lch = conv_taps.shape
+    rows, feats = tokens.shape
+    width, chans = feats * tp, lch * tp
+    pieces = 2
+    half_rows = rows // 2
+    window = half_rows + 32 * layers
+    most = window - 32
+    stat_rows = -(-most // 128) * 128
+    m = n // 2
+    dims = (n, tp, layers, ntaps, rows, width, chans, pieces)
+    vmem = pl.BlockSpec(memory_space=pltpu.VMEM)
+    anys = pl.BlockSpec(memory_space=pl.ANY)
+    bf, f32 = jnp.bfloat16, jnp.float32
+    dma = lambda k: pltpu.SemaphoreType.DMA((k,))
+    ring_sems = layers * 2 * 2 * m
+    pair_sems = layers * 2 * (2 * m + 1)
+    return pl.pallas_call(
+        functools.partial(fused, dims),
+        out_shape=jax.ShapeDtypeStruct((rows, feats), bf),
+        in_specs=[vmem, vmem, anys, anys, anys, vmem, vmem, vmem, vmem],
+        out_specs=vmem,
+        scratch_shapes=[
+            pltpu.VMEM((layers, 2, 2, width, lch), bf),
+            pltpu.VMEM((layers, 2 * lch, width), bf),
+            pltpu.VMEM((2,) + conv_taps.shape, f32),
+            pltpu.VMEM((2,) + conv_bias.shape, f32),
+            pltpu.VMEM((2,) + ln_gain.shape, f32),
+            pltpu.VMEM((2,) + ln_shift.shape, f32),
+            pltpu.VMEM((window, width), bf),
+            pltpu.VMEM((window, 2 * lch), f32),
+            pltpu.VMEM((most, 2 * lch), f32),
+            pltpu.VMEM((most, 128), f32),
+            pltpu.VMEM((most, 128), f32),
+            pltpu.VMEM((most, 2 * lch), bf),
+            pltpu.VMEM((layers, most, width), bf),
+            pltpu.VMEM((layers, most, width), bf),
+            pltpu.VMEM((layers, 8, stat_rows), f32),
+            pltpu.VMEM((layers, 8, stat_rows), f32),
+            pltpu.VMEM((stat_rows, 128), f32),
+            pltpu.VMEM((half_rows, 2 * feats), bf),
+            pltpu.VMEM((half_rows, feats), bf),
+            dma(3 * layers), dma(ring_sems), dma(ring_sems), dma(pair_sems), dma(pair_sems),
+            dma(tp - 1), dma(tp - 1), dma(tp), dma(tp), dma(4), dma(4),
+            dma(layers * pieces), dma(layers * pieces), dma(layers), dma(layers),
+            dma(pieces), dma(pieces),
+        ],
+        compiler_params=pltpu.CompilerParams(
+            collective_id=0, has_side_effects=True, vmem_limit_bytes=60 * 1024 * 1024),
+    )(tokens, norm_gain, w_value, w_gate, w_out, conv_taps, conv_bias, ln_gain, ln_shift)
+
+
+def fits(mesh, tokens, conv_taps, w_out):
+    n, tp = mesh.shape["sp"], mesh.shape["tp"]
+    layers, ntaps, lch = conv_taps.shape
+    rows, feats = tokens.shape
+    sizes = [rows // 2 + 32 * (layers - 1 - i) for i in range(layers)]
+    return (tp == 4 and n % 2 == 0 and n >= 4 and ntaps % 2 == 1 and ntaps // 2 < 16
+            and w_out.shape[2] % 128 == 0 and lch % 256 == 0 and feats % 128 == 0
+            and rows % 32 == 0 and rows // 2 >= 16 * layers
+            and all(s % 32 == 0 and (s % 112 == 0 or s % 96 == 0 or s % 128 == 0) for s in sizes)
+            and layers * w_out.shape[1] * w_out.shape[2] * n * 12 <= 20 * 1024 * 1024)
+
+
 def solution(mesh):
     placed = (
         P("sp", "tp"),
@@ -81,4 +513,10 @@
         P(None, "tp"),
         P(None, "tp", "sp"),
     )
-    return jax.shard_map(body, mesh=mesh, in_specs=placed, out_specs=P("sp", "tp"), check_vma=False)
+
+    def run(*args):
+        if fits(mesh, args[0], args[4], args[8]):
+            return fused_call(mesh, *args)
+        return body(*args)
+
+    return jax.shard_map(run, mesh=mesh, in_specs=placed, out_specs=P("sp", "tp"), check_vma=False)

time: 408 us -> 159 us (0.39)
  waiting for transfers between devices: 319 us -> 0 us
  Pallas kernels: 0 us -> 157 us
  matrix products: 22.1 us -> 0 us
  blocking collectives: 18.4 us -> 0 us
  other arithmetic: 16.2 us -> 0 us
  starting transfers between devices: 13.6 us -> 0 us
  between operations: 13.5 us -> 0.01 us
    all_gather x6 -> x0, waiting for transfers between devices: 221 us -> none  [the longest x1 60.4 us: body(): lax.all_gather(w_gate, 'sp', axis=1, tiled=True)]
    pallas_call x0 -> x1, Pallas kernels: none -> 157 us  [fused_call(): pl.pallas_call(functools.partial(fused, dims), out_shape=jax.ShapeDtypeSt...]
    reduce_scatter x3 -> x0, waiting for transfers between devices: 82.6 us -> none  [body(): lax.psum_scatter(partial_rows.astype(jnp.bfloat16), 'tp', scatter_dimensi...]
    dot_general x9 -> x0, matrix products: 22.1 us -> none  [the longest x3 9.16 us: body(): jnp.dot(activated, whole_out[layer_index], preferred_element_type=jnp.flo...]
    psum x3 -> x0, blocking collectives: 18.4 us -> none  [body(): lax.psum((jnp.sum(convolved, axis=-1, keepdims=True), jnp.sum(convolved *...]
    ppermute x6 -> x0, starting transfers between devices: 13.3 us -> none  [the longest x3 9.21 us: with_halo(): before = lax.ppermute(last, axis, up)]
    ppermute x6 -> x0, waiting for transfers between devices: 12.9 us -> none  [the longest x3 12.8 us: with_halo(): after = lax.ppermute(first, axis, down)]
    reduce_sum x6 -> x0, other arithmetic: 10.4 us -> none  [the longest x3 5.37 us: body(): jnp.mean(rows_f32 * rows_f32, axis=-1, keepdims=True) + norm_floor]
  transfers between devices with their start and end apart: 15 -> 0, of which waited for: 12 -> 0; matrix products, arithmetic and copies ran while one was open for 3% -> 0% of each run, Pallas kernels for 0% -> 0%
where the time goes in v1:
time: 159 us; the launch traced here: 158 us
  Pallas kernels  157 us (99%)
  local copies, waits for them, and re-layouts  1.77 us (1%)
    pallas_call x1, Pallas kernels, fused_call(): pl.pallas_call(functools.partial(fused, dims), out_shape=jax.ShapeDtypeSt...  157 us

profile of v1, /device:TPU:0, one launch (start us, length us, event | category | flops | bytes accessed | tf_op | source)
XLA Modules:
  0.0 158.4 jit_solution(9714775299130889978)
XLA Ops:
  0.0 156.6 %shard_map.91 = bf16[384,512]{1,0:T(8,128)(2,1)} custom-call(bf16[384,512]{1,0:T(8,128)(2,1)} %tok.1, f32[3,2048]{1,0:T(4,128)} %gain_in.1, bf16[3,256,256]{2,1,0:T(8,128)(2,1)} %wv_in.1, bf16[3,256,256]{2,1,0:T(8,128)(2,1)} %wg_in.1, bf16[3,256,256]{2,1,0:T(8,128)(2,1)} %wo_in.1, f32[3,31,256]{2,1,0:T(8,128)} %taps_in.1, f32[3,256]{1,0:T(4,128)} %bias_in.1, ...), custom_call_target="tpu_custom_call" | custom-call | tf_op jit(solution)/shard_map/pallas_call | solution.py:457
  156.6 1.8 %copy.11 = bf16[384,512]{1,0:T(8,128)(2,1)} copy(bf16[384,512]{1,0:T(8,128)(2,1)} %shard_map.91) | data formatting | bytes 786432

commit v2 on v1

--- a/solution.py
+++ b/solution.py
@@ -75,6 +75,27 @@
     return stream
 
 
+def ring_order(layers, m):
+    order = [(0, 0, 1), (0, 1, 1)]
+    for layer in range(layers):
+        order.append((layer, 2, 1))
+        for step in range(2, m + 1):
+            order += [(layer, 0, step), (layer, 1, step)]
+        ahead = [(layer + 1, 0, 1), (layer + 1, 1, 1)] if layer + 1 < layers else []
+        for step in range(2, m + 1):
+            order.append((layer, 2, step))
+            order += ahead[:1]
+            ahead = ahead[1:]
+        order += ahead
+    if m > 2:
+        last = layers - 1
+        early = [(last, 2, step) for step in range(2, m)]
+        order = [e for e in order if e not in early]
+        for e in early:
+            order.insert(order.index((last, 1, e[2] + 1)), e)
+    return order
+
+
 def fused(
     dims,
     tok, gain_in, wv_in, wg_in, wo_in, taps_in, bias_in, lng_in, lns_in,
@@ -123,31 +144,24 @@
     greet += [(right, t), (left, t)]
 
     def block(layer, kind, origin, side, half=None):
-        if kind == 0:
-            r = pl.ds(pl.multiple_of(origin * drows, drows), drows)
-            if half is None:
-                return wvg.at[layer, side, :, r, :]
-            return wvg.at[layer, side, half, r, :]
+        part, count = (0, 1) if half is None else (half, 2)
+        if kind < 2:
+            size = drows // count
+            r = pl.ds(pl.multiple_of(origin * drows + part * size, size), size)
+            return wvg.at[layer, side, kind, r, :]
+        size = lch // count
         c = pl.ds(pl.multiple_of(origin * ocols, ocols), ocols)
-        if half is None:
-            return wo.at[layer, pl.ds(pl.multiple_of(side * lch, lch), lch), c]
-        hl = lch // 2
-        return wo.at[layer, pl.ds(pl.multiple_of(side * lch + half * hl, hl), hl), c]
-
-    def local_copies(layer, kind):
-        if kind == 0:
-            r = pl.ds(pl.multiple_of(sp * drows, drows), drows)
-            return [
-                pltpu.make_async_copy(wv_in.at[layer], wvg.at[layer, h, 0, r, :], loc_sem.at[3 * layer]),
-                pltpu.make_async_copy(wg_in.at[layer], wvg.at[layer, h, 1, r, :], loc_sem.at[3 * layer + 1]),
-            ]
-        return [pltpu.make_async_copy(wo_in.at[layer], block(layer, 1, sp, h), loc_sem.at[3 * layer + 2])]
+        return wo.at[layer, pl.ds(pl.multiple_of(side * lch + part * size, size), size), c]
+
+    def local_copy(layer, kind):
+        src = (wv_in, wg_in, wo_in)[kind].at[layer]
+        return pltpu.make_async_copy(src, block(layer, kind, sp, h), loc_sem.at[3 * layer + kind])
 
     def ring_copy(layer, kind, direction, step):
         shift = -(step - 1) if direction == 0 else step - 1
         half = direction if step == m else None
         ref = block(layer, kind, ring_sp(pos + shift), h, half)
-        i = ((layer * 2 + kind) * 2 + direction) * m + step - 1
+        i = ((layer * 3 + kind) * 2 + direction) * m + step - 1
         return pltpu.make_async_remote_copy(
             src_ref=ref, dst_ref=ref, send_sem=ring_send.at[i], recv_sem=ring_recv.at[i],
             device_id=(right if direction == 0 else left, t), device_id_type=MESH)
@@ -162,34 +176,52 @@
             ref, j = block(layer, kind, sp, side), 0
         else:
             ref, j = ring_arrival(layer, kind, direction, step, side), direction * m + step
-        i = (layer * 2 + kind) * (2 * m + 1) + j
+        i = (layer * 3 + kind) * (2 * m + 1) + j
         return pltpu.make_async_remote_copy(
             src_ref=ref, dst_ref=ref, send_sem=pair_send.at[i], recv_sem=pair_recv.at[i],
             device_id=(sp, pair), device_id_type=MESH)
 
-    def send_own(layer, kind):
-        for c in local_copies(layer, kind):
-            c.wait()
-        for d in range(2):
-            ring_copy(layer, kind, d, 1).start()
-        pair_copy(layer, kind, 0, 0, h).start()
-
-    def relay(layer, kind, step):
-        for d in range(2):
-            ref = ring_arrival(layer, kind, d, step, h)
-            i = ((layer * 2 + kind) * 2 + d) * m + step - 1
-            pltpu.make_async_remote_copy(
-                src_ref=ref, dst_ref=ref, send_sem=ring_send.at[i], recv_sem=ring_recv.at[i],
-                device_id=(right, t), device_id_type=MESH).wait_recv()
-            if step < m:
-                ring_copy(layer, kind, d, step + 1).start()
-            pair_copy(layer, kind, d, step, h).start()
-
-    def pair_wait(layer, kind):
-        pair_copy(layer, kind, 0, 0, 1 - h).wait_recv()
-        for step in range(1, m + 1):
+    sequence = ring_order(layers, m)
+    place = {e: i for i, e in enumerate(sequence)}
+    sent, handled = [0], [0]
+
+    def pump():
+        while sent[0] < len(sequence):
+            layer, kind, step = sequence[sent[0]]
+            if step > 1 and place[layer, kind, step - 1] >= handled[0]:
+                return
+            if step == 1:
+                local_copy(layer, kind).wait()
             for d in range(2):
-                pair_copy(layer, kind, d, step, 1 - h).wait_recv()
+                ring_copy(layer, kind, d, step).start()
+            if step == 1:
+                pair_copy(layer, kind, 0, 0, h).start()
+            sent[0] += 1
+
+    def advance(upto):
+        while handled[0] < min(upto, len(sequence)):
+            layer, kind, step = sequence[handled[0]]
+            for d in range(2):
+                ref = ring_arrival(layer, kind, d, step, h)
+                i = ((layer * 3 + kind) * 2 + d) * m + step - 1
+                pltpu.make_async_remote_copy(
+                    src_ref=ref, dst_ref=ref, send_sem=ring_send.at[i], recv_sem=ring_recv.at[i],
+                    device_id=(right, t), device_id_type=MESH).wait_recv()
+            handled[0] += 1
+            pump()
+            for d in range(2):
+                pair_copy(layer, kind, d, step, h).start()
+
+    def advance_by(count):
+        advance(handled[0] + count)
+
+    def need(layer, *kinds):
+        advance(max(place[layer, k, m] for k in kinds) + 1)
+        for k in kinds:
+            pair_copy(layer, k, 0, 0, 1 - h).wait_recv()
+            for step in range(1, m + 1):
+                for d in range(2):
+                    pair_copy(layer, k, d, step, 1 - h).wait_recv()
 
     tcols = pl.ds(pl.multiple_of(t * feats, feats), feats)
 
@@ -242,21 +274,19 @@
                 device_id=(sp, pair), device_id_type=MESH)
 
     for layer in range(layers):
-        for kind in range(2):
-            for c in local_copies(layer, kind):
-                c.start()
+        for kind in range(3):
+            local_copy(layer, kind).start()
     for dev in greet:
         pl.semaphore_signal(barrier, inc=1, device_id=dev, device_id_type=MESH)
     pl.semaphore_wait(barrier, len(greet))
 
+    pump()
+    for j in range(1, tp):
+        tok_copy(j).start()
     for c in halo_copies():
         c.start()
-    for j in range(1, tp):
-        tok_copy(j).start()
-    send_own(0, 0)
     for c in param_copies():
         c.start()
-    send_own(0, 1)
 
     stream[pl.ds(pl.multiple_of((1 - h) * halo, grain), main), tcols] = tok[
         pl.ds(pl.multiple_of(h * (rows - main), grain), main), :]
@@ -320,17 +350,15 @@
             src_ref=src, dst_ref=dst, send_sem=px_send.at[layer * pieces + i],
             recv_sem=px_recv.at[layer * pieces + i], device_id=(sp, across), device_id_type=MESH)
 
-    for step in range(1, m + 1):
-        relay(0, 0, step)
+    advance(max(place[0, 0, m], place[0, 1, m]) + 1)
     for j in range(1, tp):
         tok_wait(j).wait_recv()
     for owner in range(tp):
         halo_wait(owner).wait_recv()
-    pair_wait(0, 0)
-    if layers > 1:
-        send_own(1, 0)
+    need(0, 0, 1)
     for i in range(2):
         project(0, i * (window // 2), window // 2)
+    advance_by(1)
     for c in param_waits():
         c.wait_recv()
 
@@ -339,6 +367,7 @@
         start = grain * (layer + 1)
         size = window - 2 * start
         convolve(layer, start, size)
+        advance_by(1)
         lane_id = lax.broadcasted_iota(jnp.int32, (size, 128), 1)
         s1 = jnp.sum(acc1[0:size, :], axis=-1, keepdims=True)
         s2 = jnp.sum(acc2[0:size, :], axis=-1, keepdims=True)
@@ -346,15 +375,12 @@
         mine = jnp.transpose(stat_m[...])
         stat_out[layer] = mine[0:8, :]
         stat_copy(layer).start()
-        for step in range(1, m + 1):
-            relay(layer, 1, step)
-        if layer + 1 < layers:
-            send_own(layer + 1, 1)
+        advance(place[layer, 2, m] + 1)
         stat_copy(layer).wait_recv()
         both = stat_out[layer] + stat_in[layer]
         wide = jnp.concatenate([both, jnp.zeros((120, both.shape[1]), jnp.float32)], axis=0)
         stat_m[...] = jnp.transpose(wide)
-        pair_wait(layer, 1)
+        need(layer, 2)
         piece = size // pieces
         for i in range(pieces):
             r0 = i * piece
@@ -369,11 +395,7 @@
                 act[r0:r0 + piece, :], wo[layer], preferred_element_type=jnp.float32).astype(jnp.bfloat16)
             part_copy(layer, i, r0, piece, last).start()
         if not last:
-            for step in range(1, m + 1):
-                relay(layer + 1, 0, step)
-            pair_wait(layer + 1, 0)
-            if layer + 2 < layers:
-                send_own(layer + 2, 0)
+            need(layer + 1, 0, 1)
             for i in range(pieces):
                 r0 = i * piece
                 part_copy(layer, i, r0, piece, last).wait_recv()
@@ -383,6 +405,7 @@
                     + part_out[layer, r0:r0 + piece, :].astype(jnp.float32)
                     + part_in[layer, r0:r0 + piece, :].astype(jnp.float32)).astype(jnp.bfloat16)
                 project(layer + 1, w0, piece)
+                advance_by(1)
         else:
             mycols = pl.ds(pl.multiple_of(xg * half_feats, half_feats), half_feats)
 
@@ -427,7 +450,7 @@
         stat_copy(layer).wait_send()
         for i in range(pieces):
             part_copy(layer, i, i * piece, piece, last).wait_send()
-        for kind in range(2):
+        for kind in range(3):
             pair_copy(layer, kind, 0, 0, h).wait_send()
             for step in range(1, m + 1):
                 for d in range(2):
@@ -452,8 +475,8 @@
     anys = pl.BlockSpec(memory_space=pl.ANY)
     bf, f32 = jnp.bfloat16, jnp.float32
     dma = lambda k: pltpu.SemaphoreType.DMA((k,))
-    ring_sems = layers * 2 * 2 * m
-    pair_sems = layers * 2 * (2 * m + 1)
+    ring_sems = layers * 3 * 2 * m
+    pair_sems = layers * 3 * (2 * m + 1)
     return pl.pallas_call(
         functools.partial(fused, dims),
         out_shape=jax.ShapeDtypeStruct((rows, feats), bf),

time: 159 us -> 132 us (0.83)
  Pallas kernels: 157 us -> 130 us
    pallas_call x1, Pallas kernels: 157 us -> 130 us  [fused_call(): pl.pallas_call(functools.partial(fused, dims), out_shape=jax.ShapeDtypeSt...]
where the time goes in v2:
time: 132 us
  Pallas kernels  130 us (98%)
  local copies, waits for them, and re-layouts  1.77 us (1%)
    pallas_call x1, Pallas kernels, fused_call(): pl.pallas_call(functools.partial(fused, dims), out_shape=jax.ShapeDtypeSt...  130 us

profile of v2, /device:TPU:0, one launch (start us, length us, event | category | flops | bytes accessed | tf_op | source)
XLA Modules:
  0.0 131.7 jit_solution(10450175615457337056)
XLA Ops:
  0.0 129.9 %shard_map.91 = bf16[384,512]{1,0:T(8,128)(2,1)} custom-call(bf16[384,512]{1,0:T(8,128)(2,1)} %tok.1, f32[3,2048]{1,0:T(4,128)} %gain_in.1, bf16[3,256,256]{2,1,0:T(8,128)(2,1)} %wv_in.1, bf16[3,256,256]{2,1,0:T(8,128)(2,1)} %wg_in.1, bf16[3,256,256]{2,1,0:T(8,128)(2,1)} %wo_in.1, f32[3,31,256]{2,1,0:T(8,128)} %taps_in.1, f32[3,256]{1,0:T(4,128)} %bias_in.1, ...), custom_call_target="tpu_custom_call" | custom-call | tf_op jit(solution)/shard_map/pallas_call | solution.py:480
  130.0 1.8 %copy.11 = bf16[384,512]{1,0:T(8,128)(2,1)} copy(bf16[384,512]{1,0:T(8,128)(2,1)} %shard_map.91) | data formatting | bytes 786432

commit v3 on v2

--- a/solution.py
+++ b/solution.py
@@ -89,7 +89,7 @@
         order += ahead
     if m > 2:
         last = layers - 1
-        early = [(last, 2, step) for step in range(2, m)]
+        early = [(last, 2, step) for step in range(2, m - 1)]
         order = [e for e in order if e not in early]
         for e in early:
             order.insert(order.index((last, 1, e[2] + 1)), e)
@@ -139,8 +139,9 @@
     up, down = lax.rem(sp + 1, n), lax.rem(sp + n - 1, n)
 
     barrier = pltpu.get_barrier_semaphore()
+    has_up, has_down = 1 - (sp + 1) // n, 1 - (n - sp) // n
+    has_halo = (1 - h) * has_down + h * has_up
     greet = [(sp, lax.rem(t + j, tp)) for j in range(1, tp)]
-    greet += [(up, j) for j in range(tp)] + [(down, j) for j in range(tp)]
     greet += [(right, t), (left, t)]
 
     def block(layer, kind, origin, side, half=None):
@@ -244,22 +245,51 @@
             src_ref=ref, dst_ref=ref, send_sem=tok_send.at[j - 1], recv_sem=tok_recv.at[j - 1],
             device_id=(sp, pair), device_id_type=MESH)
 
-    def halo_copies():
-        for g in range(tp // 2):
-            yield pltpu.make_async_remote_copy(
-                src_ref=tok.at[pl.ds(rows - halo, halo), :], dst_ref=stream.at[pl.ds(0, halo), tcols],
-                send_sem=halo_send.at[2 * g], recv_sem=halo_recv.at[t],
-                device_id=(up, 2 * g), device_id_type=MESH)
-            yield pltpu.make_async_remote_copy(
-                src_ref=tok.at[pl.ds(0, halo), :], dst_ref=stream.at[pl.ds(main, halo), tcols],
-                send_sem=halo_send.at[2 * g + 1], recv_sem=halo_recv.at[t],
-                device_id=(down, 2 * g + 1), device_id_type=MESH)
-
-    def halo_wait(owner):
-        ref = stream.at[pl.ds(pl.multiple_of(h * main, grain), halo), owner * feats:(owner + 1) * feats]
-        return pltpu.make_async_remote_copy(
-            src_ref=ref, dst_ref=ref, send_sem=halo_send.at[0], recv_sem=halo_recv.at[owner],
-            device_id=(sp, pair), device_id_type=MESH)
+    def greet_halo(there, row):
+        @pl.when(there == 1)
+        def _():
+            for c in range(2):
+                pl.semaphore_signal(barrier, inc=1, device_id=(row, 2 * xg + c), device_id_type=MESH)
+
+    def halo_copy(side):
+        src, row, there = ((rows - halo, 0, up), (0, main, down))[side]
+        return pltpu.make_async_remote_copy(
+            src_ref=tok.at[pl.ds(src, halo), :], dst_ref=stream.at[pl.ds(row, halo), tcols],
+            send_sem=halo_send.at[side], recv_sem=halo_recv.at[t],
+            device_id=(there, 2 * xg + side), device_id_type=MESH)
+
+    def halo_pass(group, c):
+        owner = 2 * group + c
+        ref = stream.at[pl.ds(pl.multiple_of(h * main, grain), halo), window_cols(owner)]
+        return pltpu.make_async_remote_copy(
+            src_ref=ref, dst_ref=ref, send_sem=halo_send.at[2 + c], recv_sem=halo_recv.at[owner],
+            device_id=(sp, across), device_id_type=MESH)
+
+    def halo_start():
+        for side, there in enumerate((has_up, has_down)):
+            pl.when(there == 1)(lambda side=side: halo_copy(side).start())
+
+    def halo_forward():
+        @pl.when(has_halo == 1)
+        def _():
+            for c in range(2):
+                halo_pass(xg, c).wait_recv()
+                halo_pass(xg, c).start()
+
+        @pl.when(has_halo == 0)
+        def _():
+            stream[pl.ds(pl.multiple_of(h * main, grain), halo), :] = jnp.zeros((halo, width), jnp.bfloat16)
+
+    def halo_finish():
+        @pl.when(has_halo == 1)
+        def _():
+            for c in range(2):
+                halo_pass(1 - xg, c).wait_recv()
+                halo_pass(xg, c).wait_send()
+
+    def halo_sent():
+        for side, there in enumerate((has_up, has_down)):
+            pl.when(there == 1)(lambda side=side: halo_copy(side).wait_send())
 
     def param_copies():
         for i, (a, b) in enumerate(((taps_in, taps), (bias_in, bias), (lng_in, lng), (lns_in, lns))):
@@ -278,13 +308,14 @@
             local_copy(layer, kind).start()
     for dev in greet:
         pl.semaphore_signal(barrier, inc=1, device_id=dev, device_id_type=MESH)
-    pl.semaphore_wait(barrier, len(greet))
+    greet_halo(has_up, up)
+    greet_halo(has_down, down)
+    pl.semaphore_wait(barrier, len(greet) + 2 * (has_up + has_down))
 
     pump()
     for j in range(1, tp):
         tok_copy(j).start()
-    for c in halo_copies():
-        c.start()
+    halo_start()
     for c in param_copies():
         c.start()
 
@@ -311,7 +342,7 @@
             g = (value * jax.nn.sigmoid(gate)).astype(jnp.bfloat16).astype(jnp.float32)
             gated[pl.ds(start, size), c * lch:(c + 1) * lch] = jnp.where(inside, g, 0.0)
 
-    def convolve(layer, start, size):
+    def convolve(layer, start, r0, size):
         lanes_per = 128
         per_side = lch // lanes_per
         acc1[...] = jnp.zeros_like(acc1)
@@ -321,18 +352,24 @@
             c = b // per_side
             lane = pl.ds(pl.multiple_of(lax.rem(b, per_side) * lanes_per, lanes_per), lanes_per)
             wide = pl.ds(pl.multiple_of(b * lanes_per, lanes_per), lanes_per)
-            for r0 in range(0, size, 112 if size % 112 == 0 else (96 if size % 96 == 0 else 128)):
-                rs = 112 if size % 112 == 0 else (96 if size % 96 == 0 else 128)
-                total = jnp.zeros((rs, lanes_per), jnp.float32) + bias[c, layer:layer + 1, lane]
-                for k in range(ntaps):
-                    total = total + taps[c, layer, k:k + 1, lane] * gated[
-                        start + r0 + k - reach:start + r0 + k - reach + rs, wide]
-                conv[r0:r0 + rs, wide] = total
-                acc1[r0:r0 + rs, :] += total
-                acc2[r0:r0 + rs, :] += total * total
+            total = jnp.zeros((size, lanes_per), jnp.float32) + bias[c, layer:layer + 1, lane]
+            for k in range(ntaps):
+                first = start + r0 + k - reach
+                total = total + taps[c, layer, k:k + 1, lane] * gated[first:first + size, wide]
+            conv[r0:r0 + size, wide] = total
+            acc1[0:size, :] += total
+            acc2[0:size, :] += total * total
             return carry
 
         lax.fori_loop(0, 2 * per_side, lane_block, 0)
+
+    def send_stats(layer, i, size):
+        lane_id = lax.broadcasted_iota(jnp.int32, (size, 128), 1)
+        s1 = jnp.sum(acc1[0:size, :], axis=-1, keepdims=True)
+        s2 = jnp.sum(acc2[0:size, :], axis=-1, keepdims=True)
+        stat_m[0:size, :] = jnp.where(lane_id == 0, s1, jnp.where(lane_id == 1, s2, 0.0))
+        stat_out[layer * pieces + i] = jnp.transpose(stat_m[...])[0:8, :]
+        stat_copy(layer * pieces + i).start()
 
     def stat_copy(layer):
         return pltpu.make_async_remote_copy(
@@ -350,11 +387,31 @@
             src_ref=src, dst_ref=dst, send_sem=px_send.at[layer * pieces + i],
             recv_sem=px_recv.at[layer * pieces + i], device_id=(sp, across), device_id_type=MESH)
 
+    def finish_sends():
+        halo_sent()
+        for j in range(1, tp):
+            tok_copy(j).wait_send()
+        for c in param_copies():
+            c.wait_send()
+        for layer in range(layers):
+            piece = (window - 2 * grain * (layer + 1)) // pieces
+            for i in range(pieces):
+                stat_copy(layer * pieces + i).wait_send()
+                if layer < layers - 1:
+                    part_copy(layer, i, i * piece, piece, False).wait_send()
+            for kind in range(3):
+                pair_copy(layer, kind, 0, 0, h).wait_send()
+                for step in range(1, m + 1):
+                    for d in range(2):
+                        ring_copy(layer, kind, d, step).wait_send()
+                        pair_copy(layer, kind, d, step, h).wait_send()
+
+    advance(3)
+    halo_forward()
     advance(max(place[0, 0, m], place[0, 1, m]) + 1)
     for j in range(1, tp):
         tok_wait(j).wait_recv()
-    for owner in range(tp):
-        halo_wait(owner).wait_recv()
+    halo_finish()
     need(0, 0, 1)
     for i in range(2):
         project(0, i * (window // 2), window // 2)
@@ -366,26 +423,21 @@
         last = layer == layers - 1
         start = grain * (layer + 1)
         size = window - 2 * start
-        convolve(layer, start, size)
-        advance_by(1)
-        lane_id = lax.broadcasted_iota(jnp.int32, (size, 128), 1)
-        s1 = jnp.sum(acc1[0:size, :], axis=-1, keepdims=True)
-        s2 = jnp.sum(acc2[0:size, :], axis=-1, keepdims=True)
-        stat_m[0:size, :] = jnp.where(lane_id == 0, s1, jnp.where(lane_id == 1, s2, 0.0))
-        mine = jnp.transpose(stat_m[...])
-        stat_out[layer] = mine[0:8, :]
-        stat_copy(layer).start()
-        advance(place[layer, 2, m] + 1)
-        stat_copy(layer).wait_recv()
-        both = stat_out[layer] + stat_in[layer]
-        wide = jnp.concatenate([both, jnp.zeros((120, both.shape[1]), jnp.float32)], axis=0)
-        stat_m[...] = jnp.transpose(wide)
-        need(layer, 2)
         piece = size // pieces
         for i in range(pieces):
+            convolve(layer, start, i * piece, piece)
+            send_stats(layer, i, piece)
+            advance_by(1)
+        need(layer, 2)
+        for i in range(pieces):
             r0 = i * piece
-            average = stat_m[r0:r0 + piece, 0:1] / chans
-            spread = stat_m[r0:r0 + piece, 1:2] / chans - average * average
+            j = layer * pieces + i
+            stat_copy(j).wait_recv()
+            both = stat_out[j] + stat_in[j]
+            wide = jnp.concatenate([both, jnp.zeros((120, both.shape[1]), jnp.float32)], axis=0)
+            sums = jnp.transpose(wide)
+            average = sums[0:piece, 0:1] / chans
+            spread = sums[0:piece, 1:2] / chans - average * average
             scale = lax.rsqrt(spread + norm_floor)
             for c in range(2):
                 y = (conv[r0:r0 + piece, c * lch:(c + 1) * lch] - average) * scale
@@ -407,6 +459,7 @@
                 project(layer + 1, w0, piece)
                 advance_by(1)
         else:
+            finish_sends()
             mycols = pl.ds(pl.multiple_of(xg * half_feats, half_feats), half_feats)
 
             def fin_copy(i, r0):
@@ -436,26 +489,8 @@
             out[pl.ds(pl.multiple_of((1 - h) * half_rows, grain), half_rows), :] = final_in[...]
             for i in range(pieces):
                 fin_copy(i, i * piece).wait_send()
-
-    for c in halo_copies():
-        c.wait_send()
-    for j in range(1, tp):
-        tok_copy(j).wait_send()
-    for c in param_copies():
-        c.wait_send()
-    for layer in range(layers):
-        last = layer == layers - 1
-        size = window - 2 * grain * (layer + 1)
-        piece = size // pieces
-        stat_copy(layer).wait_send()
-        for i in range(pieces):
-            part_copy(layer, i, i * piece, piece, last).wait_send()
-        for kind in range(3):
-            pair_copy(layer, kind, 0, 0, h).wait_send()
-            for step in range(1, m + 1):
-                for d in range(2):
-                    ring_copy(layer, kind, d, step).wait_send()
-                    pair_copy(layer, kind, d, step, h).wait_send()
+    for i in range(pieces):
+        part_copy(layers - 1, i, i * (half_rows // pieces), half_rows // pieces, True).wait_send()
 
 
 def fused_call(mesh, *args):
@@ -468,7 +503,7 @@
     half_rows = rows // 2
     window = half_rows + 32 * layers
     most = window - 32
-    stat_rows = -(-most // 128) * 128
+    stat_rows = -(-most // pieces // 128) * 128
     m = n // 2
     dims = (n, tp, layers, ntaps, rows, width, chans, pieces)
     vmem = pl.BlockSpec(memory_space=pltpu.VMEM)
@@ -492,19 +527,19 @@
             pltpu.VMEM((window, width), bf),
             pltpu.VMEM((window, 2 * lch), f32),
             pltpu.VMEM((most, 2 * lch), f32),
-            pltpu.VMEM((most, 128), f32),
-            pltpu.VMEM((most, 128), f32),
+            pltpu.VMEM((most // pieces, 128), f32),
+            pltpu.VMEM((most // pieces, 128), f32),
             pltpu.VMEM((most, 2 * lch), bf),
             pltpu.VMEM((layers, most, width), bf),
             pltpu.VMEM((layers, most, width), bf),
-            pltpu.VMEM((layers, 8, stat_rows), f32),
-            pltpu.VMEM((layers, 8, stat_rows), f32),
+            pltpu.VMEM((layers * pieces, 8, stat_rows), f32),
+            pltpu.VMEM((layers * pieces, 8, stat_rows), f32),
             pltpu.VMEM((stat_rows, 128), f32),
             pltpu.VMEM((half_rows, 2 * feats), bf),
             pltpu.VMEM((half_rows, feats), bf),
             dma(3 * layers), dma(ring_sems), dma(ring_sems), dma(pair_sems), dma(pair_sems),
             dma(tp - 1), dma(tp - 1), dma(tp), dma(tp), dma(4), dma(4),
-            dma(layers * pieces), dma(layers * pieces), dma(layers), dma(layers),
+            dma(layers * pieces), dma(layers * pieces), dma(layers * pieces), dma(layers * pieces),
             dma(pieces), dma(pieces),
         ],
         compiler_params=pltpu.CompilerParams(
@@ -520,7 +555,7 @@
     return (tp == 4 and n % 2 == 0 and n >= 4 and ntaps % 2 == 1 and ntaps // 2 < 16
             and w_out.shape[2] % 128 == 0 and lch % 256 == 0 and feats % 128 == 0
             and rows % 32 == 0 and rows // 2 >= 16 * layers
-            and all(s % 32 == 0 and (s % 112 == 0 or s % 96 == 0 or s % 128 == 0) for s in sizes)
+            and all(s % 32 == 0 and s <= 256 for s in sizes)
             and layers * w_out.shape[1] * w_out.shape[2] * n * 12 <= 20 * 1024 * 1024)
 
 

time: 132 us -> 126 us (0.955)
  Pallas kernels: 130 us -> 124 us
    pallas_call x1, Pallas kernels: 130 us -> 124 us  [fused_call(): pl.pallas_call(functools.partial(fused, dims), out_shape=jax.ShapeDtypeSt...]
where the time goes in v3:
time: 126 us; the launch traced here: 125 us
  Pallas kernels  124 us (98%)
  local copies, waits for them, and re-layouts  1.77 us (1%)
    pallas_call x1, Pallas kernels, fused_call(): pl.pallas_call(functools.partial(fused, dims), out_shape=jax.ShapeDtypeSt...  124 us

profile of v3, /device:TPU:0, one launch (start us, length us, event | category | flops | bytes accessed | tf_op | source)
XLA Modules:
  0.0 125.4 jit_solution(5265567282380650817)
XLA Ops:
  0.0 123.7 %shard_map.91 = bf16[384,512]{1,0:T(8,128)(2,1)} custom-call(bf16[384,512]{1,0:T(8,128)(2,1)} %tok.1, f32[3,2048]{1,0:T(4,128)} %gain_in.1, bf16[3,256,256]{2,1,0:T(8,128)(2,1)} %wv_in.1, bf16[3,256,256]{2,1,0:T(8,128)(2,1)} %wg_in.1, bf16[3,256,256]{2,1,0:T(8,128)(2,1)} %wo_in.1, f32[3,31,256]{2,1,0:T(8,128)} %taps_in.1, f32[3,256]{1,0:T(4,128)} %bias_in.1, ...), custom_call_target="tpu_custom_call" | custom-call | tf_op jit(solution)/shard_map/pallas_call | solution.py:515
  123.7 1.8 %copy.11 = bf16[384,512]{1,0:T(8,128)(2,1)} copy(bf16[384,512]{1,0:T(8,128)(2,1)} %shard_map.91) | data formatting | bytes 786432
